TPU v7x, 32 devices: a whole 2x2x4 slice. The times are simulated.
32 devices in a mesh: sp: 16 (over z, y, core), dp: 2 (over x).
Axes of the slice: x: 2, y: 2, z: 4, core: 2. Of those that a mesh axis runs over, the one named last changes fastest.
Arguments:
- signal: bfloat16 [2, 2048, 1024], P('dp', 'sp'), may hold values from -6 to 6
- pace: float32 [2, 16], P('dp'), may hold values from 0.5 to 2
- log_step: float32 [64], P('sp'), may hold values from -5.52 to -4.42
- a_real: float32 [64, 64], P('sp'), may hold values from -4 to -0.002, as said below
- a_imag: float32 [64, 64], P('sp'), may hold values from 0.5 to 201.06177
- in_map: float32 [64, 2, 64, 16], P('sp'), may hold values from -3 to 3
- out_map: float32 [64, 2, 16, 64], P('sp'), may hold values from -0.5 to 0.5
- skip: float32 [1024], P('sp'), may hold values from -1 to 1
- init_state: float32 [2, 2, 64, 64], P('dp', None, 'sp'), may hold values from -5 to 5
- w_glu: bfloat16 [1024, 1024], P('sp', 'dp'), may hold values from -0.1875 to 0.1875
- b_glu: float32 [1024], replicated, may hold values from -4 to 4
- g_mix: float32 [1024], replicated, may hold values from 0.1 to 1.9
- w_out: bfloat16 [1024, 4096], P('sp', 'dp'), may hold values from -0.1875 to 0.1875
Outputs:
- result: bfloat16 [2, 2048, 4096], P('dp', 'sp')
Inputs may be any that keep to these rules, and one draw needn't show every extreme that they name: `a_real`: negative entries; within a group all entries are of one order.
All inputs are finite; a program needn't handle non-finite values.
Results may differ from a plain program's by a relative error of at most 0.0075.
Values may be sent and summed in bfloat16 or wider, within the bound.
A program may use at most 64 MiB of HBM per device.

v0:
```python
import jax
import jax.numpy as jnp
from jax import lax
from jax.sharding import PartitionSpec as P


def combine(first, second):
    a1r, a1i, b1r, b1i = first
    a2r, a2i, b2r, b2i = second
    return (
        a2r * a1r - a2i * a1i,
        a2r * a1i + a2i * a1r,
        a2r * b1r - a2i * b1i + b2r,
        a2r * b1i + a2i * b1r + b2i,
    )


def mix_group(series, pace_row, log_rate, a_re, a_im, in_map, out_map, skip_row, init):
    blocks_count = pace_row.shape[0]
    length = series.shape[0]
    span = length // blocks_count
    states = a_re.shape[0]
    steps = (jnp.exp(log_rate) * pace_row)[:, None]
    decay = jnp.exp(a_re * steps)
    bar_re = decay * jnp.cos(a_im * steps)
    bar_im = decay * jnp.sin(a_im * steps)
    modulus = a_re * a_re + a_im * a_im
    coef_re = ((bar_re - 1.0) * a_re + bar_im * a_im) / modulus
    coef_im = (bar_im * a_re - (bar_re - 1.0) * a_im) / modulus
    drive_re = coef_re[..., None] * in_map[0] - coef_im[..., None] * in_map[1]
    drive_im = coef_re[..., None] * in_map[1] + coef_im[..., None] * in_map[0]
    drive = jnp.concatenate([drive_re, drive_im], axis=1).astype(jnp.bfloat16)
    blocks = series.reshape(blocks_count, span, series.shape[1])
    inject = jnp.einsum("kpc,ksc->kps", drive, blocks, preferred_element_type=jnp.float32)
    inner_re = inject[:, :states]
    inner_im = inject[:, states:]
    power_re = bar_re[..., None]
    power_im = bar_im[..., None]
    offset = 1
    while offset < span:
        moved_re = jnp.pad(inner_re[..., :-offset], ((0, 0), (0, 0), (offset, 0)))
        moved_im = jnp.pad(inner_im[..., :-offset], ((0, 0), (0, 0), (offset, 0)))
        inner_re, inner_im = (
            inner_re + power_re * moved_re - power_im * moved_im,
            inner_im + power_re * moved_im + power_im * moved_re,
        )
        power_re, power_im = (power_re * power_re - power_im * power_im, 2.0 * power_re * power_im)
        offset = offset * 2
    ends_re = (
        inner_re[:, :, -1].at[0].add(power_re[0, :, 0] * init[0] - power_im[0, :, 0] * init[1])
    )
    ends_im = (
        inner_im[:, :, -1].at[0].add(power_re[0, :, 0] * init[1] + power_im[0, :, 0] * init[0])
    )
    carried = lax.associative_scan(
        combine, (power_re[..., 0], power_im[..., 0], ends_re, ends_im), axis=0
    )
    before_re = jnp.concatenate([init[0][None], carried[2][:-1]], axis=0)[..., None]
    before_im = jnp.concatenate([init[1][None], carried[3][:-1]], axis=0)[..., None]
    places = (jnp.arange(span, dtype=jnp.float32) + 1.0)[None, None, :]
    scaled = steps[:, :, None] * places
    magnitude = jnp.exp(a_re[None, :, None] * scaled)
    angle = a_im[None, :, None] * scaled
    lift_re = magnitude * jnp.cos(angle)
    lift_im = magnitude * jnp.sin(angle)
    state_re = inner_re + lift_re * before_re - lift_im * before_im
    state_im = inner_im + lift_re * before_im + lift_im * before_re
    highest = lax.Precision.HIGHEST
    response = jnp.einsum("cp,kps->ksc", out_map[0], state_re, precision=highest) - jnp.einsum(
        "cp,kps->ksc", out_map[1], state_im, precision=highest
    )
    response = response.reshape(length, series.shape[1]) + skip_row * series.astype(jnp.float32)
    return jax.nn.gelu(response).astype(jnp.bfloat16)


def folder(left, piece):
    return jnp.dot(left, piece, preferred_element_type=jnp.float32)


def per_device(
    signal,
    pace,
    log_step,
    a_real,
    a_imag,
    in_map,
    out_map,
    skip,
    init_state,
    w_glu,
    b_glu,
    g_mix,
    w_out,
):
    local_seqs = signal.shape[0]
    tokens = signal.shape[1]
    width = signal.shape[2]
    groups = a_real.shape[0]
    channels = width // (groups * lax.axis_size("sp"))
    grouped = lax.all_to_all(signal, "sp", split_axis=2, concat_axis=1, tiled=True)
    length = grouped.shape[1]
    skips = skip.reshape(groups, channels)

    def per_sequence(inputs):
        sample, pace_row, init_row = inputs
        series = sample.reshape(length, groups, channels)
        outputs = jax.vmap(mix_group, in_axes=(1, None, 0, 0, 0, 0, 0, 0, 1), out_axes=1)(
            series, pace_row, log_step, a_real, a_imag, in_map, out_map, skips, init_row
        )
        return outputs.reshape(length, groups * channels)

    local_act = lax.map(per_sequence, (grouped, pace, init_state))
    activated = lax.all_to_all(local_act, "sp", split_axis=1, concat_axis=2, tiled=True)
    rows = activated.reshape(local_seqs * tokens, width)
    glu_cols, out_cols = (
        lax.all_gather(w_glu, "dp", axis=1, tiled=True),
        lax.all_gather(w_out, "dp", axis=1, tiled=True),
    )
    gate_pre = folder(rows, lax.all_gather(glu_cols, "sp", axis=0, tiled=True)) + b_glu
    gated = rows.astype(jnp.float32) * jax.nn.sigmoid(gate_pre)
    scale = lax.rsqrt(jnp.mean(gated * gated, axis=-1, keepdims=True) + 1e-06)
    mixed = (gated * scale * g_mix).astype(jnp.bfloat16)
    output = folder(mixed, lax.all_gather(out_cols, "sp", axis=0, tiled=True)).astype(jnp.bfloat16)
    return output.reshape(local_seqs, tokens, output.shape[1])


def solution(mesh):
    in_specs = (
        P("dp", "sp", None),
        P("dp", None),
        P("sp"),
        P("sp", None),
        P("sp", None),
        P("sp", None, None, None),
        P("sp", None, None, None),
        P("sp"),
        P("dp", None, "sp", None),
        P("sp", "dp"),
        P(),
        P(),
        P("sp", "dp"),
    )
    out_specs = P("dp", "sp", None)
    return jax.shard_map(
        per_device, mesh=mesh, in_specs=in_specs, out_specs=out_specs, check_vma=False
    )
```

profile of v0, /device:TPU:0, one launch (start us, length us, event | category | flops | bytes accessed | tf_op | source)
XLA Modules:
  0.0 147.8 jit_solution(5512769175658030008)
XLA Ops:
  6.5 7.8 %all_gather.12 = bf16[64,1024]{1,0:T(8,128)(2,1)} all-gather(bf16[64,512]{1,0:T(8,128)(2,1)} %param.26), channel_id=1, replica_groups=mesh['sp'=16,'dp'=2] {'dp'}, dimensions={1}, use_global_device_ids=true | all-gather | bytes 196608 | tf_op jit(solution)/shard_map/all_gather | solution.py:116
  14.4 8.4 %all_gather.14 = bf16[64,4096]{1,0:T(8,128)(2,1)} all-gather(bf16[64,2048]{1,0:T(8,128)(2,1)} %param.29), channel_id=1, replica_groups=mesh['sp'=16,'dp'=2] {'dp'}, dimensions={1}, use_global_device_ids=true | all-gather | bytes 786432 | tf_op jit(solution)/shard_map/all_gather | solution.py:117
  22.8 1.3 copy.90
  24.6 2.2 %reduce.14 = bf16[1024,128]{1,0:T(8,128)(2,1)S(1)} reduce(bf16[1024,1,128]{2,1,0:T(2,128)(2,1)S(1)} %bitcast.149, bf16[]{:T(256)} %broadcast.764), dimensions={1}, to_apply=%bitcast.92.reduce_sub_computation | reduce | bytes 524290
  26.8 0.8 reshape.452
  27.5 6.2 %all-to-all-start = ((bf16[16,2,4096]{2,1,0:T(2,128)(2,1)}), bf16[16,2,4096]{2,1,0:T(2,128)(2,1)S(1)}, u32[]{:S(2)}, u32[]{:S(2)}) async-start(bf16[16,2,4096]{2,1,0:T(2,128)(2,1)} %reshape.452), calls=%async_computation | async-start | bytes 524288 | tf_op jit(solution)/shard_map/all_to_all | solution.py:100
  35.7 8.1 %all-to-all-done = bf16[16,2,4096]{2,1,0:T(2,128)(2,1)S(1)} async-done(((bf16[16,2,4096]{2,1,0:T(2,128)(2,1)}), bf16[16,2,4096]{2,1,0:T(2,128)(2,1)S(1)}, u32[]{:S(2)}, u32[]{:S(2)}) %all-to-all-start) | async-done | bytes 262176 | tf_op jit(solution)/shard_map/all_to_all | solution.py:100
  44.4 1.4 fusion.48
  46.5 2.5 %fusion.4 = (f32[4,16,64,128]{3,2,1,0:T(8,128)S(1)}, f32[4,16,64,128]{3,2,1,0:T(8,128)S(1)}) fusion(f32[4,16,128,128]{3,2,1,0:T(8,128)S(1)} %fusion.48, f32[4,16,64,127]{3,2,1,0:T(8,128)S(1)} %get-tuple-element.102, f32[4,16,64,127]{3,2,1,0:T(8,128)S(1)} %get-tuple-element.101, f32[4,16,64]{2,1,0:T(8,128)S(1)} %get-tuple-element.151, ...), kind=kLoop, calls=%fused_computation.11 | loop fusion | flops 4194304 | bytes 12582912 | tf_op jit(solution)/shard_map/while/body/eval_jaxpr/vmap()/sub | solution.py:44
  49.0 2.5 %multiply_subtract_fusion.5 = (f32[4,16,64,128]{3,2,1,0:T(8,128)S(1)}, f32[4,16,64,128]{3,2,1,0:T(8,128)S(1)}) fusion(f32[4,16,64,128]{3,2,1,0:T(8,128)S(1)} %get-tuple-element.87, f32[4,16,64,126]{3,2,1,0:T(8,128)S(1)} %bitcast.135, f32[4,16,64,126]{3,2,1,0:T(8,128)S(1)} %bitcast.134, f32[4,16,64]{2,1,0:T(8,128)S(1)} %get-tuple-element.152, ...), kind=kLoop, calls=%fused_computation.34 | loop fusion | flops 4194304 | bytes 12550144 | tf_op jit(solution)/shard_map/while/body/eval_jaxpr/vmap()/sub | solution.py:44
  51.5 2.5 %multiply_subtract_fusion.4 = (f32[4,16,64,128]{3,2,1,0:T(8,128)S(1)}, f32[4,16,64,128]{3,2,1,0:T(8,128)S(1)}) fusion(f32[4,16,64,128]{3,2,1,0:T(8,128)S(1)} %get-tuple-element.99, f32[4,16,64,124]{3,2,1,0:T(8,128)S(1)} %bitcast.139, f32[4,16,64,124]{3,2,1,0:T(8,128)S(1)} %bitcast.138, f32[4,16,64]{2,1,0:T(8,128)S(1)} %get-tuple-element.148, ...), kind=kLoop, calls=%fused_computation.32 | loop fusion | flops 4194304 | bytes 12484608 | tf_op jit(solution)/shard_map/while/body/eval_jaxpr/vmap()/sub | solution.py:44
  54.1 2.5 %multiply_subtract_fusion.3 = (f32[4,16,64,128]{3,2,1,0:T(8,128)S(1)}, f32[4,16,64,128]{3,2,1,0:T(8,128)S(1)}) fusion(f32[4,16,64,128]{3,2,1,0:T(8,128)S(1)} %get-tuple-element.97, f32[4,16,64,120]{3,2,1,0:T(8,128)S(1)} %bitcast.141, f32[4,16,64,120]{3,2,1,0:T(8,128)S(1)} %bitcast.140, f32[4,16,64]{2,1,0:T(8,128)S(1)} %get-tuple-element.146, ...), kind=kLoop, calls=%fused_computation.30 | loop fusion | flops 4194304 | bytes 12353536 | tf_op jit(solution)/shard_map/while/body/eval_jaxpr/vmap()/sub | solution.py:44
  56.6 2.5 %multiply_subtract_fusion.2 = (f32[4,16,64,128]{3,2,1,0:T(8,128)S(1)}, f32[4,16,64,128]{3,2,1,0:T(8,128)S(1)}) fusion(f32[4,16,64,128]{3,2,1,0:T(8,128)S(1)} %get-tuple-element.95, f32[4,16,64,112]{3,2,1,0:T(8,128)S(1)} %bitcast.143, f32[4,16,64,112]{3,2,1,0:T(8,128)S(1)} %bitcast.142, f32[4,16,64]{2,1,0:T(8,128)S(1)} %get-tuple-element.144, ...), kind=kLoop, calls=%fused_computation.28 | loop fusion | flops 4194304 | bytes 12091392 | tf_op jit(solution)/shard_map/while/body/eval_jaxpr/vmap()/sub | solution.py:44
  59.1 2.5 %multiply_subtract_fusion.1 = (f32[4,16,64,128]{3,2,1,0:T(8,128)S(1)}, f32[4,16,64,128]{3,2,1,0:T(8,128)S(1)}) fusion(f32[4,16,64,128]{3,2,1,0:T(8,128)S(1)} %get-tuple-element.93, f32[4,16,64,96]{3,2,1,0:T(8,128)S(1)} %bitcast.145, f32[4,16,64,96]{3,2,1,0:T(8,128)S(1)} %bitcast.144, f32[4,16,64]{2,1,0:T(8,128)S(1)} %get-tuple-element.142, ...), kind=kLoop, calls=%fused_computation.26 | loop fusion | flops 4194304 | bytes 11567104 | tf_op jit(solution)/shard_map/while/body/eval_jaxpr/vmap()/sub | solution.py:44
  61.7 2.5 %multiply_subtract_fusion = (f32[4,16,64,128]{3,2,1,0:T(8,128)S(1)}, f32[4,16,64,128]{3,2,1,0:T(8,128)S(1)}) fusion(f32[4,16,64,128]{3,2,1,0:T(8,128)S(1)} %get-tuple-element.91, f32[4,16,64,64]{3,2,1,0:T(8,128)S(1)} %bitcast.137, f32[4,16,64,64]{3,2,1,0:T(8,128)S(1)} %bitcast.136, f32[4,16,64]{2,1,0:T(8,128)S(1)} %get-tuple-element.140, ...), kind=kLoop, calls=%fused_computation.24 | loop fusion | flops 4194304 | bytes 10518528 | tf_op jit(solution)/shard_map/while/body/eval_jaxpr/vmap()/sub | solution.py:44
  64.5 2.2 %slice_reduce_fusion = (f32[4,16,64]{2,1,0:T(8,128)S(1)}, f32[4,16,64]{2,1,0:T(8,128)S(1)}) fusion(f32[4,16,64,128]{3,2,1,0:T(8,128)S(1)} %get-tuple-element.90, f32[4,16,64,128]{3,2,1,0:T(8,128)S(1)} %get-tuple-element.89), kind=kLoop, calls=%fused_computation.6 | loop fusion | bytes 65536 | tf_op jit(solution)/shard_map/while/body/eval_jaxpr/vmap()/slice | solution.py:53
  68.6 11.0 %fusion.5 = f32[4,16,128,16]{2,3,1,0:T(8,128)S(1)} fusion(f32[4,16,64,128]{3,2,1,0:T(8,128)} %copy-done, f32[4,16,64]{2,1,0:T(8,128)S(1)} %pad_maximum_fusion.1, f32[4,16,64]{2,1,0:T(8,128)S(1)} %pad_maximum_fusion, f32[4,64]{1,0:T(4,128)S(1)} %copy-done.3, f32[4,16,128]{2,1,0:T(8,128)S(1)} %broadcast_multiply_fusion.6, f32[4,64]{1,0:T(4,128)S(1)} %copy-done.4, ...), kind=kOutput, calls=%fused_computation.12 | convolution fusion | flops 104857600 | bytes 2756608 | tf_op jit(solution)/shard_map/while/body/eval_jaxpr/vmap(cp,kps->ksc)/dot_general | solution.py:69
  79.6 9.9 %fusion.22 = f32[4,16,2,8,128]{4,3,2,1,0:T(8,128)S(1)} fusion(f32[4,16,128,16]{2,3,1,0:T(8,128)S(1)} %fusion.5, f32[4,16,64,128]{3,2,1,0:T(8,128)S(1)} %get-tuple-element.89, f32[4,16,64]{2,1,0:T(8,128)S(1)} %pad_maximum_fusion.1, f32[4,16,64]{2,1,0:T(8,128)S(1)} %pad_maximum_fusion, f32[4,64]{1,0:T(4,128)S(1)} %copy-done.3, ...), kind=kOutput, calls=%fused_computation.36 | convolution fusion | flops 104988672 | bytes 3280896 | tf_op jit(solution)/shard_map/while/body/eval_jaxpr/vmap(cp,kps->ksc)/dot_general | solution.py:69
  89.9 0.7 copy.127
  90.6 11.4 %reduce.15 = bf16[2048,64]{1,0:T(8,128)(2,1)S(1)} reduce(bf16[2048,1,64]{2,1,0:T(2,128)(2,1)S(1)} %bitcast.147, bf16[]{:T(256)} %broadcast.764), dimensions={1}, to_apply=%bitcast.94.reduce_sub_computation | reduce | bytes 524290
  102.5 20.1 %all_to_all.30 = bf16[16,2,4096]{2,1,0:T(2,128)(2,1)S(1)} all-to-all(bf16[16,2,4096]{2,1,0:T(2,128)(2,1)S(1)} %reshape.454), channel_id=1, replica_groups=mesh['sp'=16,'dp'=2] {'sp'}, dimensions={0} | all-to-all | bytes 524288 | tf_op jit(solution)/shard_map/all_to_all | solution.py:113
  124.2 2.2 %multiply_reduce_fusion = (f32[128]{0:T(128)S(1)}, f32[128,1024]{1,0:T(8,128)S(1)}) fusion(f32[1024]{0:T(1024)S(1)} %copy-done.9, bf16[128,1024]{0,1:T(8,128)(2,1)S(1)} %bitcast.153, bf16[1024,1024]{1,0:T(8,128)(2,1)} %all-gather.3.cloned.1.call-done, bf16[128,1024]{1,0:T(8,128)(2,1)S(1)} %copy.130), kind=kOutput, calls=%fused_computation.64 | convolution fusion | flops 269483904 | bytes 3150336 | tf_op jit(solution)/shard_map/dot_general | solution.py:77
  126.4 8.8 %all-gather.5.cloned.1.call-done = bf16[1024,4096]{1,0:T(8,128)(2,1)} async-done(((bf16[64,4096]{1,0:T(8,128)(2,1)}), bf16[1024,4096]{1,0:T(8,128)(2,1)}) %all-gather.5.cloned.1.call-update) | async-done | bytes 8388624 | tf_op jit(solution)/shard_map/all_gather | solution.py:123
  135.3 5.7 %fusion = bf16[1,128,4096]{2,1,0:T(8,128)(2,1)} fusion(bf16[1024,4096]{1,0:T(8,128)(2,1)} %all-gather.5.cloned.1.call-done, f32[128,1024]{1,0:T(8,128)S(1)} %get-tuple-element.161, f32[1024]{0:T(1024)S(1)} %copy-done.1, f32[128]{0:T(128)S(1)} %add_rsqrt_fusion), kind=kOutput, calls=%fused_computation.1 | convolution fusion | flops 1074659328 | bytes 9966080 | tf_op jit(solution)/shard_map/dot_general | solution.py:77
  (140 shorter events, 7.7 us)
Async XLA Ops:
  6.5 27.2 %copy-start.10 = (f32[4]{0:T(128)S(1)}, f32[4]{0:T(128)}, u32[]{:S(2)}) copy-start(f32[4]{0:T(128)} %param.19) | copy-start | bytes 52
  6.5 27.2 %copy-start.7 = (f32[1,16]{1,0:T(1,128)S(1)}, f32[1,16]{1,0:T(1,128)}, u32[]{:S(2)}) copy-start(f32[1,16]{1,0:T(1,128)} %param.18) | copy-start | bytes 196
  6.5 27.4 %copy-start.4 = (f32[4,64]{1,0:T(4,128)S(1)}, f32[4,64]{1,0:T(4,128)}, u32[]{:S(2)}) copy-start(f32[4,64]{1,0:T(4,128)} %param.20) | copy-start | bytes 3076
  6.5 117.6 %all-gather.3.cloned.1.call-start = ((), (), s32[]{:S(2)}) async-start(), calls=%async_computation.2 | async-start | bytes 2228224 | tf_op jit(solution)/shard_map/all_gather | solution.py:119
  14.3 19.7 %copy-start.3 = (f32[4,64]{1,0:T(4,128)S(1)}, f32[4,64]{1,0:T(4,128)}, u32[]{:S(2)}) copy-start(f32[4,64]{1,0:T(4,128)} %param.21) | copy-start | bytes 3076
  14.3 120.9 %all-gather.5.cloned.1.call-start = ((), (), s32[]{:S(2)}) async-start(), calls=%async_computation.3 | async-start | bytes 8912896 | tf_op jit(solution)/shard_map/all_gather | solution.py:123
  24.1 11.3 %copy-start.5 = (f32[1,2,4,64]{3,2,1,0:T(4,128)S(1)}, f32[1,2,4,64]{3,2,1,0:T(4,128)}, u32[]{:S(2)}) copy-start(f32[1,2,4,64]{3,2,1,0:T(4,128)} %param.25) | copy-start | bytes 6148
  24.6 10.9 %copy-start.6 = (f32[64]{0:T(128)S(1)}, f32[64]{0:T(128)}, u32[]{:S(2)}) copy-start(f32[64]{0:T(128)} %param.24) | copy-start | bytes 772
  24.6 11.0 %copy-start.2 = (f32[4,2,64,16]{2,3,1,0:T(8,128)S(1)}, f32[4,2,64,16]{2,3,1,0:T(8,128)}, u32[]{:S(2)}) copy-start(f32[4,2,64,16]{2,3,1,0:T(8,128)} %param.22) | copy-start | bytes 98308
  27.5 16.3 %all-to-all-start = ((bf16[16,2,4096]{2,1,0:T(2,128)(2,1)}), bf16[16,2,4096]{2,1,0:T(2,128)(2,1)S(1)}, u32[]{:S(2)}, u32[]{:S(2)}) async-start(bf16[16,2,4096]{2,1,0:T(2,128)(2,1)} %reshape.452), calls=%async_computation | async-start | bytes 524288 | tf_op jit(solution)/shard_map/all_to_all | solution.py:100
  64.2 2.6 %copy-start = (f32[4,16,64,128]{3,2,1,0:T(8,128)}, f32[4,16,64,128]{3,2,1,0:T(8,128)S(1)}, u32[]{:S(2)}) copy-start(f32[4,16,64,128]{3,2,1,0:T(8,128)S(1)} %get-tuple-element.90) | copy-start | bytes 6291460
  66.7 1.8 %copy-start.8 = (f32[4,2,16,64]{3,2,1,0:T(8,128)S(1)}, f32[4,2,16,64]{3,2,1,0:T(8,128)}, u32[]{:S(2)}) copy-start(f32[4,2,16,64]{3,2,1,0:T(8,128)} %param.23) | copy-start | bytes 98308
  122.6 1.6 %copy-start.9 = (f32[1024]{0:T(1024)S(1)}, f32[1024]{0:T(1024)}, u32[]{:S(2)}) copy-start(f32[1024]{0:T(1024)} %param.27) | copy-start | bytes 12292
  124.1 11.2 %copy-start.1 = (f32[1024]{0:T(1024)S(1)}, f32[1024]{0:T(1024)}, u32[]{:S(2)}) copy-start(f32[1024]{0:T(1024)} %param.28) | copy-start | bytes 12292
Sparse Core Ops, SparseCore 0:
  14.5 41.9 all-gather.2
  58.6 76.6 all-gather.4
where the time goes:
time: 148 us
  blocking collectives  36.3 us (25%)
  other arithmetic  33.4 us (23%)
  matrix products  30.3 us (20%)
  waiting for transfers between devices  17 us (11%)
  between operations  14.1 us (10%)
  local copies, waits for them, and re-layouts  10.5 us (7%)
  starting transfers between devices  6.23 us (4%)
    all_to_all x1, blocking collectives, per_device(): lax.all_to_all(local_act, 'sp', split_axis=1, concat_axis=2, tiled=True)  20.1 us
    sub x7, other arithmetic, mix_group(): inner_re + power_re * moved_re - power_im * moved_im  17.7 us
    unnamed x2, other arithmetic  13.6 us
    dot_general x1, matrix products, mix_group(): jnp.einsum('cp,kps->ksc', out_map[1], state_im, precision=highest)  11 us
    dot_general x1, matrix products, mix_group(): jnp.einsum('cp,kps->ksc', out_map[0], state_re, precision=highest)  9.95 us
    all_gather x1, waiting for transfers between devices, per_device(): lax.all_gather(out_cols, 'sp', axis=0, tiled=True)  8.84 us
    all_gather x1, blocking collectives, per_device(): lax.all_gather(w_out, 'dp', axis=1, tiled=True)  8.38 us
    all_to_all x1, waiting for transfers between devices, per_device(): lax.all_to_all(signal, 'sp', split_axis=2, concat_axis=1, tiled=True)  8.07 us
  transfers between devices with their start and end apart: 3, of which 2 were waited for; matrix products, arithmetic and copies ran while one was open for 46% of the time, Pallas kernels for 0%

commit v1 on v0

v1 whole, which is shorter than its diff:
```python
import functools
import math

import jax
import jax.numpy as jnp
from jax import lax
from jax.experimental import pallas as pl
from jax.experimental.pallas import tpu as pltpu
from jax.sharding import PartitionSpec as P

F32 = jnp.float32
BF16 = jnp.bfloat16
MESH = pl.DeviceIdType.MESH
LANES = 128
ORDERS = (("x", "y", "z"), ("y", "x", "z"), ("z", "y", "x"), ("z", "x", "y"))


def cmul(ar, ai, br, bi):
    return ar * br - ai * bi, ar * bi + ai * br


def powers(br, bi, count):
    row = lax.broadcasted_iota(jnp.int32, (8, br.shape[1]), 0)
    pr = jnp.ones((8, br.shape[1]), F32)
    pi = jnp.zeros((8, br.shape[1]), F32)
    sr, si = br, bi
    for bit in (1, 2, 4):
        qr, qi = cmul(pr, pi, sr, si)
        on = (row & bit) != 0
        pr, pi = jnp.where(on, qr, pr), jnp.where(on, qi, pi)
        sr, si = cmul(sr, si, sr, si)
    size = 8
    while size < count:
        qr, qi = cmul(pr, pi, sr, si)
        pr = jnp.concatenate([pr, qr], axis=0)
        pi = jnp.concatenate([pi, qi], axis=0)
        sr, si = cmul(sr, si, sr, si)
        size *= 2
    return pr, pi


def gelu(v):
    return 0.5 * v * (1.0 + jnp.tanh(math.sqrt(2.0 / math.pi) * (v + 0.044715 * (v * v * v))))


def kernel(
    dims, sizes,
    sig, par, pace, inm, outm, skips, b_glu, g_mix, wg_hbm, wo_hbm, out,
    buf0, buf1, buf2, buf3, tx, rx, atx, arx, bars, cmat,
    lsem, wsend, wrecv, xsend, xrecv, asend, arecv,
):
    n_sp, n_dp, tokens, wd, fold, rows, states = sizes
    bufs = (buf0, buf1, buf2, buf3)
    me = lax.axis_index("sp")
    mx = lax.axis_index("dp")
    nc, ny, nz = dims["c"], dims["y"], dims["z"]
    at = {"x": mx, "c": lax.rem(me, nc), "y": lax.rem(me // nc, ny), "z": me // (nc * ny)}
    gcols = wg_hbm.shape[1] // 4
    ocols = wo_hbm.shape[1] // 4

    def device(where):
        return {"sp": (where["z"] * ny + where["y"]) * nc + where["c"], "dp": where["x"]}

    def slot(t, where, level):
        order = ORDERS[t]
        index = [where["c"]] + [where[order[i]] for i in (2, 1, 0)][: 3 - level]
        return bufs[t].at[tuple(index)]

    local = []
    for t in range(4):
        own = slot(t, at, 0)
        local.append(pltpu.make_async_copy(
            wo_hbm.at[:, pl.ds(t * ocols, ocols)], own.at[:, pl.ds(0, ocols)], lsem.at[2 * t]))
        if gcols % LANES:
            own[:, ocols:] = wg_hbm[:, t * gcols:(t + 1) * gcols]
        else:
            local.append(pltpu.make_async_copy(
                wg_hbm.at[:, pl.ds(t * gcols, gcols)], own.at[:, pl.ds(ocols, gcols)], lsem.at[2 * t + 1]))
    for copy in local:
        copy.start()

    barrier = pltpu.get_barrier_semaphore()

    def greet(d, carry):
        pl.semaphore_signal(barrier, 1, device_id={"sp": lax.rem(me + d, n_sp), "dp": mx}, device_id_type=MESH)
        return carry

    lax.fori_loop(1, n_sp, greet, 0)
    for d in range(1, n_dp):
        pl.semaphore_signal(barrier, 1, device_id={"sp": me, "dp": lax.rem(mx + d, n_dp)}, device_id_type=MESH)

    part = lax.broadcasted_iota(jnp.int32, (rows, LANES), 1) // wd
    for tile in range(sig.shape[1] // LANES):
        pieces = [
            sig[p * rows:(p + 1) * rows, tile * LANES:(tile + 1) * LANES].astype(F32) for p in range(fold)
        ]
        for j in range(fold):
            acc = pieces[j]
            for p in range(fold):
                if p != j:
                    moved = pltpu.roll(pieces[p], ((p - j) * wd) % LANES, 1)
                    acc = jnp.where(part == p, moved, acc)
            tx[tile * fold + j] = acc.astype(BF16)

    pl.semaphore_wait(barrier, n_sp - 1 + n_dp - 1)

    def chunk_copy(src, dst, ssem, rsem, to, frm):
        return pltpu.make_async_remote_copy(
            src_ref=src, dst_ref=dst, send_sem=ssem.at[to], recv_sem=rsem.at[frm],
            device_id={"sp": to, "dp": mx}, device_id_type=MESH)

    def send_chunk(d, carry):
        to = lax.rem(me + d, n_sp)
        chunk_copy(tx.at[to], rx.at[me], xsend, xrecv, to, me).start()
        return carry

    lax.fori_loop(1, n_sp, send_chunk, 0)

    pending = []
    counter = [0]

    def post(src, where):
        k = counter[0]
        counter[0] += 1
        copy = pltpu.make_async_remote_copy(
            src_ref=src, dst_ref=src, send_sem=wsend.at[k], recv_sem=wrecv.at[k],
            device_id=device(where), device_id_type=MESH)
        copy.start()
        pending.append(copy)
        return k

    def arrive(k, dst):
        pltpu.make_async_remote_copy(
            src_ref=dst, dst_ref=dst, send_sem=wsend.at[k], recv_sem=wrecv.at[k],
            device_id=device(at), device_id_type=MESH).wait_recv()

    last = []

    def sibling(t, where, level):
        for d in range(1, nc):
            to = dict(at, c=lax.rem(at["c"] + d, nc))
            frm = dict(where, c=lax.rem(at["c"] + nc - d, nc))
            k = post(slot(t, where, level), to)
            last.append((k, slot(t, frm, level)))

    def start_stage(t, level):
        axis = ORDERS[t][level]
        n = dims[axis]
        posted = []
        ring = level == 2 and n == 4 and dims[ORDERS[t][1]] % 2 == 0
        for d in ((1, 3) if ring else range(1, n)):
            k = post(slot(t, at, level), dict(at, **{axis: lax.rem(at[axis] + d, n)}))
            posted.append((k, dict(at, **{axis: lax.rem(at[axis] + n - d, n)}), d))
        return posted

    def end_stage(t, level, posted):
        axis = ORDERS[t][level]
        n = dims[axis]
        ring = level == 2 and n == 4 and dims[ORDERS[t][1]] % 2 == 0
        halves = []
        for k, where, d in posted:
            arrive(k, slot(t, where, level))
            if ring:
                half = dims[ORDERS[t][1]] // 2
                span = pl.ds(0 if d == 1 else half, half)
                k2 = post(slot(t, where, level).at[span], dict(at, **{axis: lax.rem(at[axis] + d, n)}))
                halves.append((k2, span))
            if level > 0:
                sibling(t, where, level)
        if level == 0:
            sibling(t, at, 1)
        return halves

    def end_ring(t, halves):
        axis = ORDERS[t][2]
        where = dict(at, **{axis: lax.rem(at[axis] + 2, 4)})
        for k, span in halves:
            arrive(k, slot(t, where, 2).at[span])
        if halves:
            sibling(t, where, 2)

    for copy in local:
        copy.wait()
    stage = {t: start_stage(t, 0) for t in range(4)}

    a_re, a_im, log_step = par[0:1], par[1:2], par[2:3]
    steps = pace[...] * jnp.exp(log_step)
    real, angle = a_re * steps, a_im * steps
    decay, growth = jnp.exp(real), jnp.exp(-real)
    cos, sin = jnp.cos(angle), jnp.sin(angle)
    bar_re, bar_im = decay * cos, decay * sin
    modulus = a_re * a_re + a_im * a_im
    bars[0] = bar_re
    bars[1] = bar_im
    bars[2] = growth * cos
    bars[3] = -growth * sin
    bars[4] = ((bar_re - 1.0) * a_re + bar_im * a_im) / modulus
    bars[5] = (bar_im * a_re - (bar_re - 1.0) * a_im) / modulus
    for p in range(fold):
        for j in range(2):
            blank = [jnp.zeros((wd, states), BF16)] * fold
            blank[p] = outm[j].astype(BF16)
            cmat[2 * p + j] = jnp.concatenate(blank, axis=0)

    for t in range(4):
        end_stage(t, 0, stage[t])
        stage[t] = start_stage(t, 1)

    rx[me] = tx[me]

    def take_chunk(d, carry):
        frm = lax.rem(me + n_sp - d, n_sp)
        chunk_copy(tx.at[me], rx.at[frm], xsend, xrecv, me, frm).wait_recv()
        return carry

    lax.fori_loop(1, n_sp, take_chunk, 0)

    span_row = lax.broadcasted_iota(jnp.int32, (tokens, tokens), 0)
    span_col = lax.broadcasted_iota(jnp.int32, (tokens, tokens), 1)
    tri = jnp.where(span_row >= span_col, 1.0, 0.0).astype(BF16)
    dot = functools.partial(jnp.dot, preferred_element_type=F32)

    def dot_t(a, b):
        return lax.dot_general(a, b, (((1,), (1,)), ((), ())), preferred_element_type=F32)

    def block(k, carry):
        before_re, before_im = carry
        br, bi, gr, gi, cr, ci = [bars[j, pl.ds(k, 1), :] for j in range(6)]
        chunk = rx[k]
        drive_re = (cr * inm[0] - ci * inm[1]).astype(BF16)
        drive_im = (cr * inm[1] + ci * inm[0]).astype(BF16)
        zero = jnp.zeros_like(drive_re)

        def inject(drive):
            return jnp.concatenate(
                [dot(chunk, jnp.concatenate([drive if q == p else zero for q in range(fold)], axis=0))
                 for p in range(fold)], axis=0)

        up_re, up_im = powers(gr, gi, tokens)
        sum_re, sum_im = cmul(inject(drive_re), inject(drive_im), up_re, up_im)
        sum_re, sum_im = dot(tri, sum_re.astype(BF16)), dot(tri, sum_im.astype(BF16))
        first_re, first_im = cmul(br, bi, before_re, before_im)
        down_re, down_im = powers(br, bi, tokens)
        state_re, state_im = cmul(sum_re + first_re, sum_im + first_im, down_re, down_im)
        s_re, s_im = state_re.astype(BF16), state_im.astype(BF16)
        response = skips[...] * chunk.astype(F32)
        for p in range(fold):
            lines = slice(p * rows, (p + 1) * rows)
            response = response + dot_t(s_re[lines], cmat[2 * p]) - dot_t(s_im[lines], cmat[2 * p + 1])
        atx[k] = gelu(response).astype(BF16)

        @pl.when(k != me)
        def _():
            chunk_copy(atx.at[k], arx.at[me], asend, arecv, k, me).start()

        return state_re[tokens - 1:], state_im[tokens - 1:]

    carry = (par[3:4], par[4:5])
    cuts = [n_sp * i // 4 for i in range(5)]
    halves = {}
    for s in range(4):
        carry = lax.fori_loop(cuts[s], cuts[s + 1], block, carry)
        if s == 0:
            for t in range(4):
                end_stage(t, 1, stage[t])
                stage[t] = start_stage(t, 2)
        if s == 2:
            for t in (0, 1):
                halves[t] = end_stage(t, 2, stage[t])
    for t in (2, 3):
        halves[t] = end_stage(t, 2, stage[t])

    arx[me] = atx[me]

    def take_act(d, carry):
        frm = lax.rem(me + n_sp - d, n_sp)
        chunk_copy(atx.at[me], arx.at[frm], asend, arecv, me, frm).wait_recv()
        return carry

    lax.fori_loop(1, n_sp, take_act, 0)
    tiles = []
    for tile in range(sig.shape[1] // LANES):
        chunks = [arx[tile * fold + j].astype(F32) for j in range(fold)]
        parts = []
        for p in range(fold):
            acc = chunks[p]
            for j in range(fold):
                if j != p:
                    moved = pltpu.roll(chunks[j], ((j - p) * wd) % LANES, 1)
                    acc = jnp.where(part == j, moved, acc)
            parts.append(acc)
        tiles.append(jnp.concatenate(parts, axis=0))
    act = jnp.concatenate(tiles, axis=1)
    act_bf = act.astype(BF16)

    for t in range(4):
        end_ring(t, halves[t])
    for k, dst in last:
        arrive(k, dst)

    def weight(t, x, cols):
        order = ORDERS[t]
        found = []
        for i in range(n_sp):
            where = {"x": x, "c": i % nc, "y": (i // nc) % ny, "z": i // (nc * ny)}
            index = (where["c"],) + tuple(where[order[i2]] for i2 in (2, 1, 0))
            found.append(bufs[t][index + (slice(None), cols)])
        return jnp.concatenate(found, axis=0)

    gate = jnp.concatenate(
        [dot(act_bf, weight(t, x, slice(ocols, ocols + gcols))) for x in range(n_dp) for t in range(4)], axis=1)
    gated = act * jax.nn.sigmoid(gate + b_glu[...])
    scale = lax.rsqrt(jnp.mean(gated * gated, axis=-1, keepdims=True) + 1e-06)
    mixed = (gated * scale * g_mix[...]).astype(BF16)
    for x in range(n_dp):
        for t in range(4):
            at_col = (x * 4 + t) * ocols
            out[:, at_col:at_col + ocols] = dot(mixed, weight(t, x, slice(0, ocols))).astype(BF16)

    def drain(d, carry):
        to = lax.rem(me + d, n_sp)
        chunk_copy(tx.at[to], rx.at[me], xsend, xrecv, to, me).wait_send()
        chunk_copy(atx.at[to], arx.at[me], asend, arecv, to, me).wait_send()
        return carry

    lax.fori_loop(1, n_sp, drain, 0)
    for copy in pending:
        copy.wait_send()


def per_device(
    signal, pace, log_step, a_real, a_imag, in_map, out_map, skip, init_state, w_glu, b_glu, g_mix, w_out
):
    n_sp, n_dp = lax.axis_size("sp"), lax.axis_size("dp")
    tokens, width = signal.shape[1], signal.shape[2]
    groups, entries = a_real.shape
    channels = width // (groups * n_sp)
    wd = groups * channels
    states = groups * entries
    fold = LANES // wd
    rows = tokens // fold
    assert signal.shape[0] == 1 and pace.shape[1] == n_sp and n_sp % 4 == 0
    dims = {"x": n_dp, "c": 2, "y": 2, "z": n_sp // 4}
    eye = jnp.eye(groups, dtype=F32)
    inm = (in_map.transpose(1, 0, 3, 2)[:, :, :, None, :] * eye[None, :, None, :, None]).reshape(2, wd, states)
    outm = (out_map.transpose(1, 0, 2, 3)[:, :, :, None, :] * eye[None, :, None, :, None]).reshape(2, wd, states)
    par = jnp.stack([
        a_real.reshape(states), a_imag.reshape(states), jnp.repeat(log_step, entries),
        init_state[0, 0].reshape(states), init_state[0, 1].reshape(states)])
    pcols = (w_out.shape[1] + w_glu.shape[1]) // 4
    wrows = w_out.shape[0]
    copies = 0
    for order in ORDERS:
        n1, n2, n3 = [dims[a] for a in order]
        copies += (n1 - 1) + (n2 - 1) + (n3 - 1) + 1 + (n2 - 1) + (n3 - 1) + 4
    vmem = pl.BlockSpec(memory_space=pltpu.VMEM)
    hbm = pl.BlockSpec(memory_space=pl.ANY)
    chunk = pltpu.VMEM((n_sp, rows, LANES), BF16)
    sem = pltpu.SemaphoreType.DMA
    out_width = w_out.shape[1] * n_dp
    output = pl.pallas_call(
        functools.partial(kernel, dims, (n_sp, n_dp, tokens, wd, fold, rows, states)),
        out_shape=jax.ShapeDtypeStruct((tokens, out_width), BF16),
        in_specs=[vmem] * 8 + [vmem if w_glu.shape[1] % (4 * LANES) else hbm, hbm],
        out_specs=vmem,
        scratch_shapes=[
            pltpu.VMEM((2, dims[o[2]], dims[o[1]], dims[o[0]], wrows, pcols), BF16) for o in ORDERS
        ] + [chunk] * 4 + [
            pltpu.VMEM((6, n_sp, states), F32),
            pltpu.VMEM((2 * fold, LANES, states), BF16),
            sem((8,)), sem((copies,)), sem((copies,)),
            sem((n_sp,)), sem((n_sp,)), sem((n_sp,)), sem((n_sp,)),
        ],
        compiler_params=pltpu.CompilerParams(
            collective_id=0, has_side_effects=True, vmem_limit_bytes=56 * 1024 * 1024),
    )(
        signal[0], par, pace.reshape(n_sp, 1), inm, outm, jnp.tile(skip, fold)[None],
        b_glu[None], g_mix[None], w_glu, w_out)
    return output[None]


def solution(mesh):
    in_specs = (
        P("dp", "sp", None),
        P("dp", None),
        P("sp"),
        P("sp", None),
        P("sp", None),
        P("sp", None, None, None),
        P("sp", None, None, None),
        P("sp"),
        P("dp", None, "sp", None),
        P("sp", "dp"),
        P(),
        P(),
        P("sp", "dp"),
    )
    out_specs = P("dp", "sp", None)
    return jax.shard_map(
        per_device, mesh=mesh, in_specs=in_specs, out_specs=out_specs, check_vma=False
    )
```

time: 148 us -> 95.4 us (0.64)
  the two profiles are of different devices: /device:TPU:0 before, /device:TPU:29 now
where the time goes in v1:
time: 95.4 us; the launch traced here: 95 us
  Pallas kernels  84 us (88%)
  local copies, waits for them, and re-layouts  10.3 us (11%)
    pallas_call x1, Pallas kernels, per_device(): pl.pallas_call(functools.partial(kernel, dims, (n_sp, n_dp, tokens, wd, f...  84 us
    unnamed x5, local copies, waits for them, and re-layouts  3.12 us
    another operation x6, local copies, waits for them, and re-layouts, per_device(): jnp.stack([a_real.reshape(states), a_imag.reshape(states), jnp.repeat(log...  2.41 us

profile of v1, /device:TPU:29, one launch (start us, length us, event | category | flops | bytes accessed | tf_op | source)
XLA Modules:
  0.0 95.0 jit_solution(3665594615591542977)
XLA Ops:
  0.0 0.0 copy-start
  0.0 0.8 stack_reshape.9
  0.8 0.8 stack_reshape.10
  1.6 0.7 tile.2
  2.2 0.6 broadcast_in_dim_tile.3.skips
  2.8 0.7 broadcast_in_dim.16
  3.5 0.1 stack_reshape.11
  3.6 0.7 fusion.1
  4.3 0.1 stack_reshape_squeeze.7
  4.4 0.1 stack_reshape_squeeze.6
  4.5 0.6 stack.3.par
  5.1 1.3 %copy.16.pace = f32[16,1]{1,0:T(8,128)} copy(f32[16,1]{0,1:T(1,128)} %bitcast.13) | data formatting | bytes 128 | tf_op jit(solution)/shard_map/reshape | solution.py:377
  6.4 0.0 copy-done
  6.4 0.0 copy-start.1
  6.4 0.8 copy-done.1
  7.3 0.1 mul.42
  7.3 0.1 mul.43
  7.5 0.2 mul.47
  7.8 0.2 mul.41
  8.0 0.7 broadcast_multiply_fusion
  8.7 84.0 %shard_map.127 = bf16[128,4096]{1,0:T(8,128)(2,1)} custom-call(bf16[128,1024]{1,0:T(8,128)(2,1)} %bitcast.8, f32[5,256]{1,0:T(8,128)} %stack.3.par, f32[16,1]{1,0:T(8,128)} %copy.16.pace, f32[2,64,256]{2,1,0:T(8,128)} %get-tuple-element.6.inm, f32[2,64,256]{2,1,0:T(8,128)} %get-tuple-element.5.outm, f32[1,128]{1,0:T(1,128)} %broadcast_in_dim_tile.3.skips, ...), custom_call_target="tpu_custom_call" | custom-call | tf_op jit(solution)/shard_map/pallas_call | solution.py:361
  92.8 2.3 %copy.18 = bf16[1,128,4096]{2,1,0:T(8,128)(2,1)} copy(bf16[1,128,4096]{2,1,0:T(8,128)(2,1)} %bitcast.7) | data formatting | bytes 2097152
  (5 shorter events, 0.1 us)
Async XLA Ops:
  0.0 6.4 %copy-start = (f32[4,2,64,16]{2,3,1,0:T(8,128)S(1)}, f32[4,2,64,16]{2,3,1,0:T(8,128)}, u32[]{:S(2)}) copy-start(f32[4,2,64,16]{2,3,1,0:T(8,128)} %param.18) | copy-start | bytes 98308
  6.4 0.8 copy-start.1

commit v2 on v1

--- a/solution.py
+++ b/solution.py
@@ -12,7 +12,8 @@
 BF16 = jnp.bfloat16
 MESH = pl.DeviceIdType.MESH
 LANES = 128
-ORDERS = (("x", "y", "z"), ("y", "x", "z"), ("z", "y", "x"), ("z", "x", "y"))
+ORDERS = (("z", "y"), ("z", "y"), ("z", "y"), ("z", "y"), ("y", "z"))
+CUTS = len(ORDERS) - 1
 
 
 def cmul(ar, ai, br, bi):
@@ -46,36 +47,29 @@
 def kernel(
     dims, sizes,
     sig, par, pace, inm, outm, skips, b_glu, g_mix, wg_hbm, wo_hbm, out,
-    buf0, buf1, buf2, buf3, tx, rx, atx, arx, bars, cmat,
-    lsem, wsend, wrecv, xsend, xrecv, asend, arecv,
+    buf0, buf1, buf2, buf3, buf4, mrx, ostage, tx, rx, atx, arx, bars, cmat,
+    lsem, wsend, wrecv, xsend, xrecv, asend, arecv, msend, mrecv, osend, orecv,
 ):
     n_sp, n_dp, tokens, wd, fold, rows, states = sizes
-    bufs = (buf0, buf1, buf2, buf3)
+    bufs = (buf0, buf1, buf2, buf3, buf4)
     me = lax.axis_index("sp")
     mx = lax.axis_index("dp")
     nc, ny, nz = dims["c"], dims["y"], dims["z"]
     at = {"x": mx, "c": lax.rem(me, nc), "y": lax.rem(me // nc, ny), "z": me // (nc * ny)}
-    gcols = wg_hbm.shape[1] // 4
-    ocols = wo_hbm.shape[1] // 4
+    gcols = wg_hbm.shape[1]
+    ocols = wo_hbm.shape[1] // CUTS
 
     def device(where):
         return {"sp": (where["z"] * ny + where["y"]) * nc + where["c"], "dp": where["x"]}
 
-    def slot(t, where, level):
-        order = ORDERS[t]
-        index = [where["c"]] + [where[order[i]] for i in (2, 1, 0)][: 3 - level]
-        return bufs[t].at[tuple(index)]
-
-    local = []
-    for t in range(4):
-        own = slot(t, at, 0)
+    def slot(t, where):
+        index = (where["c"], where["z"], where["y"])
+        return bufs[t].at[((where["x"],) if t == 0 else ()) + index]
+
+    local = [pltpu.make_async_copy(wg_hbm, slot(0, at), lsem.at[0])]
+    for t in range(CUTS):
         local.append(pltpu.make_async_copy(
-            wo_hbm.at[:, pl.ds(t * ocols, ocols)], own.at[:, pl.ds(0, ocols)], lsem.at[2 * t]))
-        if gcols % LANES:
-            own[:, ocols:] = wg_hbm[:, t * gcols:(t + 1) * gcols]
-        else:
-            local.append(pltpu.make_async_copy(
-                wg_hbm.at[:, pl.ds(t * gcols, gcols)], own.at[:, pl.ds(ocols, gcols)], lsem.at[2 * t + 1]))
+            wo_hbm.at[:, pl.ds(t * ocols, ocols)], slot(t + 1, at), lsem.at[t + 1]))
     for copy in local:
         copy.start()
 
@@ -119,69 +113,101 @@
     pending = []
     counter = [0]
 
-    def post(src, where):
-        k = counter[0]
+    def guarded(cond, action):
+        if cond is None:
+            action()
+        else:
+            pl.when(cond)(action)
+
+    def take():
         counter[0] += 1
-        copy = pltpu.make_async_remote_copy(
-            src_ref=src, dst_ref=src, send_sem=wsend.at[k], recv_sem=wrecv.at[k],
+        return counter[0] - 1
+
+    def copy_of(k, ref, where):
+        return pltpu.make_async_remote_copy(
+            src_ref=ref, dst_ref=ref, send_sem=wsend.at[k], recv_sem=wrecv.at[k],
             device_id=device(where), device_id_type=MESH)
-        copy.start()
-        pending.append(copy)
-        return k
-
-    def arrive(k, dst):
-        pltpu.make_async_remote_copy(
-            src_ref=dst, dst_ref=dst, send_sem=wsend.at[k], recv_sem=wrecv.at[k],
-            device_id=device(at), device_id_type=MESH).wait_recv()
-
-    last = []
-
-    def sibling(t, where, level):
+
+    def post(k, ref, where, cond=None):
+        guarded(cond, lambda: copy_of(k, ref, where).start())
+        pending.append((k, ref, where, cond))
+
+    def arrive(k, ref, cond=None):
+        guarded(cond, lambda: copy_of(k, ref, at).wait_recv())
+
+    handed = {t: [] for t in range(len(ORDERS))}
+
+    def sibling(t, where, cond):
         for d in range(1, nc):
-            to = dict(at, c=lax.rem(at["c"] + d, nc))
-            frm = dict(where, c=lax.rem(at["c"] + nc - d, nc))
-            k = post(slot(t, where, level), to)
-            last.append((k, slot(t, frm, level)))
-
-    def start_stage(t, level):
-        axis = ORDERS[t][level]
-        n = dims[axis]
-        posted = []
-        ring = level == 2 and n == 4 and dims[ORDERS[t][1]] % 2 == 0
-        for d in ((1, 3) if ring else range(1, n)):
-            k = post(slot(t, at, level), dict(at, **{axis: lax.rem(at[axis] + d, n)}))
-            posted.append((k, dict(at, **{axis: lax.rem(at[axis] + n - d, n)}), d))
-        return posted
-
-    def end_stage(t, level, posted):
-        axis = ORDERS[t][level]
-        n = dims[axis]
-        ring = level == 2 and n == 4 and dims[ORDERS[t][1]] % 2 == 0
-        halves = []
-        for k, where, d in posted:
-            arrive(k, slot(t, where, level))
-            if ring:
-                half = dims[ORDERS[t][1]] // 2
-                span = pl.ds(0 if d == 1 else half, half)
-                k2 = post(slot(t, where, level).at[span], dict(at, **{axis: lax.rem(at[axis] + d, n)}))
-                halves.append((k2, span))
-            if level > 0:
-                sibling(t, where, level)
-        if level == 0:
-            sibling(t, at, 1)
-        return halves
-
-    def end_ring(t, halves):
-        axis = ORDERS[t][2]
-        where = dict(at, **{axis: lax.rem(at[axis] + 2, 4)})
-        for k, span in halves:
-            arrive(k, slot(t, where, 2).at[span])
-        if halves:
-            sibling(t, where, 2)
+            k = take()
+            post(k, slot(t, where), dict(at, c=lax.rem(at["c"] + d, nc)), cond)
+            handed[t].append((k, slot(t, dict(where, c=lax.rem(at["c"] + nc - d, nc))), cond))
+
+    def source(move):
+        where, cond = dict(at), None
+        for axis, m in move.items():
+            n, i = dims[axis], at[axis]
+            if n == 2:
+                where[axis] = 1 - i if m else i
+            elif m:
+                here = jnp.logical_and(i - m >= 0, i - m < n)
+                cond = here if cond is None else jnp.logical_and(cond, here)
+                where[axis] = jnp.clip(i - m, 0, n - 1)
+        return where, cond
+
+    def gather(t):
+        order = ORDERS[t] + (("x",) if t == 0 and n_dp == 2 else ())
+        wave = [(None, {axis: 0 for axis in order}, 0)]
+        while wave:
+            later = []
+            for k, move, level in wave:
+                where, cond = source(move)
+                if k is not None:
+                    arrive(k, slot(t, where), cond)
+                for deeper in range(level, len(order)):
+                    axis = order[deeper]
+                    n, i, m = dims[axis], at[axis], move[axis]
+                    if n == 2:
+                        ways = () if m else (1,)
+                    else:
+                        ways = (1, -1) if m == 0 else ((m // abs(m),) if abs(m) < n - 1 else ())
+                    for way in ways:
+                        k2 = take()
+                        if n == 2:
+                            to, ok = 1 - i, cond
+                        else:
+                            to, ok = jnp.clip(i + way, 0, n - 1), (i < n - 1) if way == 1 else (i > 0)
+                            ok = ok if cond is None else jnp.logical_and(ok, cond)
+                        post(k2, slot(t, where), dict(at, **{axis: to}), ok)
+                        later.append((k2, dict(move, **{axis: m + way}), deeper))
+                sibling(t, where, cond)
+            wave = later
+            yield
+        for k, ref, cond in handed[t]:
+            arrive(k, ref, cond)
+        if t == 0 and n_dp > 2:
+            swaps = []
+            for d in range(1, n_dp):
+                k = take()
+                post(k, bufs[0].at[mx], dict(at, x=lax.rem(mx + d, n_dp)))
+                swaps.append((k, lax.rem(mx + n_dp - d, n_dp)))
+            yield
+            for k, frm in swaps:
+                arrive(k, bufs[0].at[frm])
+
+    runs = {t: gather(t) for t in range(len(ORDERS))}
+
+    def advance(which=None):
+        for t in range(len(ORDERS)) if which is None else (which,):
+            next(runs[t], None)
+
+    def complete(t):
+        for _ in runs[t]:
+            pass
 
     for copy in local:
         copy.wait()
-    stage = {t: start_stage(t, 0) for t in range(4)}
+    advance()
 
     a_re, a_im, log_step = par[0:1], par[1:2], par[2:3]
     steps = pace[...] * jnp.exp(log_step)
@@ -202,10 +228,6 @@
             blank[p] = outm[j].astype(BF16)
             cmat[2 * p + j] = jnp.concatenate(blank, axis=0)
 
-    for t in range(4):
-        end_stage(t, 0, stage[t])
-        stage[t] = start_stage(t, 1)
-
     rx[me] = tx[me]
 
     def take_chunk(d, carry):
@@ -256,19 +278,11 @@
         return state_re[tokens - 1:], state_im[tokens - 1:]
 
     carry = (par[3:4], par[4:5])
-    cuts = [n_sp * i // 4 for i in range(5)]
-    halves = {}
-    for s in range(4):
+    advance()
+    cuts = [n_sp * i // 2 for i in range(3)]
+    for s in range(2):
         carry = lax.fori_loop(cuts[s], cuts[s + 1], block, carry)
-        if s == 0:
-            for t in range(4):
-                end_stage(t, 1, stage[t])
-                stage[t] = start_stage(t, 2)
-        if s == 2:
-            for t in (0, 1):
-                halves[t] = end_stage(t, 2, stage[t])
-    for t in (2, 3):
-        halves[t] = end_stage(t, 2, stage[t])
+        advance()
 
     arx[me] = atx[me]
 
@@ -293,29 +307,55 @@
     act = jnp.concatenate(tiles, axis=1)
     act_bf = act.astype(BF16)
 
-    for t in range(4):
-        end_ring(t, halves[t])
-    for k, dst in last:
-        arrive(k, dst)
-
-    def weight(t, x, cols):
-        order = ORDERS[t]
+    def weight(t, x):
         found = []
         for i in range(n_sp):
-            where = {"x": x, "c": i % nc, "y": (i // nc) % ny, "z": i // (nc * ny)}
-            index = (where["c"],) + tuple(where[order[i2]] for i2 in (2, 1, 0))
-            found.append(bufs[t][index + (slice(None), cols)])
+            index = (i % nc, i // (nc * ny), (i // nc) % ny)
+            found.append(bufs[t][((x,) if t == 0 else ()) + index])
         return jnp.concatenate(found, axis=0)
 
-    gate = jnp.concatenate(
-        [dot(act_bf, weight(t, x, slice(ocols, ocols + gcols))) for x in range(n_dp) for t in range(4)], axis=1)
+    for step in range(2 * dims["z"]):
+        advance()
+    complete(0)
+    gate = jnp.concatenate([dot(act_bf, weight(0, x)) for x in range(n_dp)], axis=1)
     gated = act * jax.nn.sigmoid(gate + b_glu[...])
     scale = lax.rsqrt(jnp.mean(gated * gated, axis=-1, keepdims=True) + 1e-06)
     mixed = (gated * scale * g_mix[...]).astype(BF16)
-    for x in range(n_dp):
-        for t in range(4):
-            at_col = (x * 4 + t) * ocols
-            out[:, at_col:at_col + ocols] = dot(mixed, weight(t, x, slice(0, ocols))).astype(BF16)
+    mrx[mx] = mixed
+
+    def mixed_copy(frm, to):
+        return pltpu.make_async_remote_copy(
+            src_ref=mrx.at[frm], dst_ref=mrx.at[frm], send_sem=msend.at[to], recv_sem=mrecv.at[frm],
+            device_id={"sp": me, "dp": to}, device_id_type=MESH)
+
+    others = [lax.rem(mx + d, n_dp) for d in range(1, n_dp)]
+    for to in others:
+        mixed_copy(mx, to).start()
+    for t in range(1, CUTS + 1):
+        complete(t)
+
+    def out_copy(frm, to, t):
+        cols = pl.ds(pl.multiple_of((frm * CUTS + t) * ocols, LANES), ocols)
+        return pltpu.make_async_remote_copy(
+            src_ref=ostage.at[to, t], dst_ref=out.at[:, cols], send_sem=osend.at[to, t],
+            recv_sem=orecv.at[frm, t], device_id={"sp": me, "dp": to}, device_id_type=MESH)
+
+    for to in others:
+        mixed_copy(to, mx).wait_recv()
+    for t in range(CUTS):
+        for to in others:
+            ostage[to, t] = dot(mrx[to], weight(t + 1, None)).astype(BF16)
+            out_copy(mx, to, t).start()
+    for t in range(CUTS):
+        cols = pl.ds(pl.multiple_of((mx * CUTS + t) * ocols, LANES), ocols)
+        out[:, cols] = dot(mixed, weight(t + 1, None)).astype(BF16)
+    for t in range(CUTS):
+        for frm in others:
+            out_copy(frm, mx, t).wait_recv()
+    for to in others:
+        mixed_copy(mx, to).wait_send()
+        for t in range(CUTS):
+            out_copy(mx, to, t).wait_send()
 
     def drain(d, carry):
         to = lax.rem(me + d, n_sp)
@@ -324,8 +364,8 @@
         return carry
 
     lax.fori_loop(1, n_sp, drain, 0)
-    for copy in pending:
-        copy.wait_send()
+    for k, ref, where, cond in pending:
+        guarded(cond, lambda: copy_of(k, ref, where).wait_send())
 
 
 def per_device(
@@ -347,12 +387,9 @@
     par = jnp.stack([
         a_real.reshape(states), a_imag.reshape(states), jnp.repeat(log_step, entries),
         init_state[0, 0].reshape(states), init_state[0, 1].reshape(states)])
-    pcols = (w_out.shape[1] + w_glu.shape[1]) // 4
     wrows = w_out.shape[0]
-    copies = 0
-    for order in ORDERS:
-        n1, n2, n3 = [dims[a] for a in order]
-        copies += (n1 - 1) + (n2 - 1) + (n3 - 1) + 1 + (n2 - 1) + (n3 - 1) + 4
+    gcols, ocols = w_glu.shape[1], w_out.shape[1] // CUTS
+    copies = 2 * (len(ORDERS) + 1) * 2 * dims["z"] * dims["y"] + n_dp
     vmem = pl.BlockSpec(memory_space=pltpu.VMEM)
     hbm = pl.BlockSpec(memory_space=pl.ANY)
     chunk = pltpu.VMEM((n_sp, rows, LANES), BF16)
@@ -361,15 +398,20 @@
     output = pl.pallas_call(
         functools.partial(kernel, dims, (n_sp, n_dp, tokens, wd, fold, rows, states)),
         out_shape=jax.ShapeDtypeStruct((tokens, out_width), BF16),
-        in_specs=[vmem] * 8 + [vmem if w_glu.shape[1] % (4 * LANES) else hbm, hbm],
+        in_specs=[vmem] * 8 + [hbm] * 2,
         out_specs=vmem,
         scratch_shapes=[
-            pltpu.VMEM((2, dims[o[2]], dims[o[1]], dims[o[0]], wrows, pcols), BF16) for o in ORDERS
+            pltpu.VMEM(((n_dp,) if t == 0 else ()) + (2, dims["z"], dims["y"], wrows, gcols if t == 0 else ocols), BF16)
+            for t in range(len(ORDERS))
+        ] + [
+            pltpu.VMEM((n_dp, tokens, width), BF16),
+            pltpu.VMEM((n_dp, CUTS, tokens, ocols), BF16),
         ] + [chunk] * 4 + [
             pltpu.VMEM((6, n_sp, states), F32),
             pltpu.VMEM((2 * fold, LANES, states), BF16),
             sem((8,)), sem((copies,)), sem((copies,)),
             sem((n_sp,)), sem((n_sp,)), sem((n_sp,)), sem((n_sp,)),
+            sem((n_dp,)), sem((n_dp,)), sem((n_dp, CUTS)), sem((n_dp, CUTS)),
         ],
         compiler_params=pltpu.CompilerParams(
             collective_id=0, has_side_effects=True, vmem_limit_bytes=56 * 1024 * 1024),

time: 95.4 us -> 84.2 us (0.88)
  the two profiles are of different devices: /device:TPU:29 before, /device:TPU:0 now
where the time goes in v2:
time: 84.2 us; the launch traced here: 83.8 us
  Pallas kernels  72.8 us (86%)
  local copies, waits for them, and re-layouts  10.3 us (12%)
    pallas_call x1, Pallas kernels, per_device(): pl.pallas_call(functools.partial(kernel, dims, (n_sp, n_dp, tokens, wd, f...  72.8 us
    unnamed x5, local copies, waits for them, and re-layouts  3.12 us
    another operation x6, local copies, waits for them, and re-layouts, per_device(): jnp.stack([a_real.reshape(states), a_imag.reshape(states), jnp.repeat(log...  2.41 us

profile of v2, /device:TPU:0, one launch (start us, length us, event | category | flops | bytes accessed | tf_op | source)
XLA Modules:
  0.0 83.8 jit_solution(14448781342319499695)
XLA Ops:
  0.0 0.0 copy-start
  0.0 0.8 stack_reshape.9
  0.8 0.8 stack_reshape.10
  1.6 0.7 tile.2
  2.2 0.6 broadcast_in_dim_tile.3.skips
  2.8 0.7 broadcast_in_dim.16
  3.5 0.1 stack_reshape.11
  3.6 0.7 fusion.1
  4.3 0.1 stack_reshape_squeeze.7
  4.4 0.1 stack_reshape_squeeze.6
  4.5 0.6 stack.3.par
  5.1 1.3 %copy.16.pace = f32[16,1]{1,0:T(8,128)} copy(f32[16,1]{0,1:T(1,128)} %bitcast.13) | data formatting | bytes 128 | tf_op jit(solution)/shard_map/reshape | solution.py:419
  6.4 0.0 copy-done
  6.4 0.0 copy-start.1
  6.4 0.8 copy-done.1
  7.3 0.1 mul.42
  7.3 0.1 mul.43
  7.5 0.2 mul.47
  7.8 0.2 mul.41
  8.0 0.7 broadcast_multiply_fusion
  8.7 72.8 %shard_map.127 = bf16[128,4096]{1,0:T(8,128)(2,1)} custom-call(bf16[128,1024]{1,0:T(8,128)(2,1)} %bitcast.8, f32[5,256]{1,0:T(8,128)} %stack.3.par, f32[16,1]{1,0:T(8,128)} %copy.16.pace, f32[2,64,256]{2,1,0:T(8,128)} %get-tuple-element.6.inm, f32[2,64,256]{2,1,0:T(8,128)} %get-tuple-element.5.outm, f32[1,128]{1,0:T(1,128)} %broadcast_in_dim_tile.3.skips, ...), custom_call_target="tpu_custom_call" | custom-call | tf_op jit(solution)/shard_map/pallas_call | solution.py:398
  81.6 2.3 %copy.18 = bf16[1,128,4096]{2,1,0:T(8,128)(2,1)} copy(bf16[1,128,4096]{2,1,0:T(8,128)(2,1)} %bitcast.7) | data formatting | bytes 2097152
  (5 shorter events, 0.1 us)
Async XLA Ops:
  0.0 6.4 %copy-start = (f32[4,2,64,16]{2,3,1,0:T(8,128)S(1)}, f32[4,2,64,16]{2,3,1,0:T(8,128)}, u32[]{:S(2)}) copy-start(f32[4,2,64,16]{2,3,1,0:T(8,128)} %param.18) | copy-start | bytes 98308
  6.4 0.8 %copy-start.1 = (f32[4,2,16,64]{3,2,1,0:T(8,128)S(1)}, f32[4,2,16,64]{3,2,1,0:T(8,128)}, u32[]{:S(2)}) copy-start(f32[4,2,16,64]{3,2,1,0:T(8,128)} %param.19) | copy-start | bytes 98308

commit v3 on v2

--- a/solution.py
+++ b/solution.py
@@ -12,8 +12,12 @@
 BF16 = jnp.bfloat16
 MESH = pl.DeviceIdType.MESH
 LANES = 128
-ORDERS = (("z", "y"), ("z", "y"), ("z", "y"), ("z", "y"), ("y", "z"))
+ORDERS = (("z", "y"),) * 5
 CUTS = len(ORDERS) - 1
+
+
+def spread_pieces(n_dp):
+    return 2 if n_dp == 2 else 1
 
 
 def cmul(ar, ai, br, bi):
@@ -46,11 +50,12 @@
 
 def kernel(
     dims, sizes,
-    sig, par, pace, inm, outm, skips, b_glu, g_mix, wg_hbm, wo_hbm, out,
+    sig, a_real, a_imag, init, in_map, out_map, log_step, pace, skip, b_glu, g_mix, wg_hbm, wo_hbm, out,
     buf0, buf1, buf2, buf3, buf4, mrx, ostage, tx, rx, atx, arx, bars, cmat,
-    lsem, wsend, wrecv, xsend, xrecv, asend, arecv, msend, mrecv, osend, orecv,
+    inm, lsem, wsend, wrecv, xsend, xrecv, asend, arecv, msend, mrecv, osend, orecv,
 ):
     n_sp, n_dp, tokens, wd, fold, rows, states = sizes
+    spread = spread_pieces(n_dp)
     bufs = (buf0, buf1, buf2, buf3, buf4)
     me = lax.axis_index("sp")
     mx = lax.axis_index("dp")
@@ -64,7 +69,7 @@
 
     def slot(t, where):
         index = (where["c"], where["z"], where["y"])
-        return bufs[t].at[((where["x"],) if t == 0 else ()) + index]
+        return bufs[t].at[((where["x"],) if t < spread else ()) + index]
 
     local = [pltpu.make_async_copy(wg_hbm, slot(0, at), lsem.at[0])]
     for t in range(CUTS):
@@ -156,7 +161,7 @@
         return where, cond
 
     def gather(t):
-        order = ORDERS[t] + (("x",) if t == 0 and n_dp == 2 else ())
+        order = ORDERS[t] + (("x",) if t < spread and n_dp == 2 else ())
         wave = [(None, {axis: 0 for axis in order}, 0)]
         while wave:
             later = []
@@ -209,8 +214,35 @@
         copy.wait()
     advance()
 
-    a_re, a_im, log_step = par[0:1], par[1:2], par[2:3]
-    steps = pace[...] * jnp.exp(log_step)
+    groups, entries = a_real.shape
+    channels = wd // groups
+    lane_group = lax.broadcasted_iota(jnp.int32, (1, states), 1) // entries
+    block_row = lax.broadcasted_iota(jnp.int32, (n_sp, states), 0)
+
+    def row_of(ref, *lead):
+        found = [ref[lead + (slice(g, g + 1), slice(None))] for g in range(groups)]
+        return jnp.concatenate(found, axis=1)
+
+    a_re, a_im = row_of(a_real), row_of(a_imag)
+    log_row = jnp.full((1, states), log_step[0], F32)
+    for g in range(1, groups):
+        log_row = jnp.where(lane_group == g, log_step[g], log_row)
+    paces = jnp.full((n_sp, states), pace[0, 0], F32)
+    for k in range(1, n_sp):
+        paces = jnp.where(block_row == k, pace[0, k], paces)
+    steps = paces * jnp.exp(log_row)
+
+    def diagonal(blocks):
+        lines = []
+        for g in range(groups):
+            line = [jnp.zeros((channels, entries), F32)] * groups
+            line[g] = blocks[g]
+            lines.append(jnp.concatenate(line, axis=1))
+        return jnp.concatenate(lines, axis=0)
+
+    for j in range(2):
+        inm[j] = diagonal([in_map[g, j] for g in range(groups)])
+    skips = jnp.concatenate([skip[...].reshape(1, wd)] * fold, axis=1)
     real, angle = a_re * steps, a_im * steps
     decay, growth = jnp.exp(real), jnp.exp(-real)
     cos, sin = jnp.cos(angle), jnp.sin(angle)
@@ -225,7 +257,7 @@
     for p in range(fold):
         for j in range(2):
             blank = [jnp.zeros((wd, states), BF16)] * fold
-            blank[p] = outm[j].astype(BF16)
+            blank[p] = diagonal([out_map[g, j] for g in range(groups)]).astype(BF16)
             cmat[2 * p + j] = jnp.concatenate(blank, axis=0)
 
     rx[me] = tx[me]
@@ -265,7 +297,7 @@
         down_re, down_im = powers(br, bi, tokens)
         state_re, state_im = cmul(sum_re + first_re, sum_im + first_im, down_re, down_im)
         s_re, s_im = state_re.astype(BF16), state_im.astype(BF16)
-        response = skips[...] * chunk.astype(F32)
+        response = skips * chunk.astype(F32)
         for p in range(fold):
             lines = slice(p * rows, (p + 1) * rows)
             response = response + dot_t(s_re[lines], cmat[2 * p]) - dot_t(s_im[lines], cmat[2 * p + 1])
@@ -277,7 +309,7 @@
 
         return state_re[tokens - 1:], state_im[tokens - 1:]
 
-    carry = (par[3:4], par[4:5])
+    carry = (row_of(init, 0, 0), row_of(init, 0, 1))
     advance()
     cuts = [n_sp * i // 2 for i in range(3)]
     for s in range(2):
@@ -311,16 +343,16 @@
         found = []
         for i in range(n_sp):
             index = (i % nc, i // (nc * ny), (i // nc) % ny)
-            found.append(bufs[t][((x,) if t == 0 else ()) + index])
+            found.append(bufs[t][((x,) if t < spread else ()) + index])
         return jnp.concatenate(found, axis=0)
 
     for step in range(2 * dims["z"]):
         advance()
     complete(0)
     gate = jnp.concatenate([dot(act_bf, weight(0, x)) for x in range(n_dp)], axis=1)
-    gated = act * jax.nn.sigmoid(gate + b_glu[...])
+    gated = act * jax.nn.sigmoid(gate + b_glu[...].reshape(1, -1))
     scale = lax.rsqrt(jnp.mean(gated * gated, axis=-1, keepdims=True) + 1e-06)
-    mixed = (gated * scale * g_mix[...]).astype(BF16)
+    mixed = (gated * scale * g_mix[...].reshape(1, -1)).astype(BF16)
     mrx[mx] = mixed
 
     def mixed_copy(frm, to):
@@ -331,7 +363,13 @@
     others = [lax.rem(mx + d, n_dp) for d in range(1, n_dp)]
     for to in others:
         mixed_copy(mx, to).start()
-    for t in range(1, CUTS + 1):
+    for t in range(1, spread):
+        complete(t)
+    for t in range(spread - 1):
+        for x in range(n_dp):
+            cols = slice((x * CUTS + t) * ocols, (x * CUTS + t + 1) * ocols)
+            out[:, cols] = dot(mixed, weight(t + 1, x)).astype(BF16)
+    for t in range(spread, CUTS + 1):
         complete(t)
 
     def out_copy(frm, to, t):
@@ -342,19 +380,20 @@
 
     for to in others:
         mixed_copy(to, mx).wait_recv()
-    for t in range(CUTS):
+    alone = range(spread - 1, CUTS)
+    for t in alone:
         for to in others:
             ostage[to, t] = dot(mrx[to], weight(t + 1, None)).astype(BF16)
             out_copy(mx, to, t).start()
-    for t in range(CUTS):
+    for t in alone:
         cols = pl.ds(pl.multiple_of((mx * CUTS + t) * ocols, LANES), ocols)
         out[:, cols] = dot(mixed, weight(t + 1, None)).astype(BF16)
-    for t in range(CUTS):
+    for t in alone:
         for frm in others:
             out_copy(frm, mx, t).wait_recv()
     for to in others:
         mixed_copy(mx, to).wait_send()
-        for t in range(CUTS):
+        for t in alone:
             out_copy(mx, to, t).wait_send()
 
     def drain(d, carry):
@@ -381,16 +420,11 @@
     rows = tokens // fold
     assert signal.shape[0] == 1 and pace.shape[1] == n_sp and n_sp % 4 == 0
     dims = {"x": n_dp, "c": 2, "y": 2, "z": n_sp // 4}
-    eye = jnp.eye(groups, dtype=F32)
-    inm = (in_map.transpose(1, 0, 3, 2)[:, :, :, None, :] * eye[None, :, None, :, None]).reshape(2, wd, states)
-    outm = (out_map.transpose(1, 0, 2, 3)[:, :, :, None, :] * eye[None, :, None, :, None]).reshape(2, wd, states)
-    par = jnp.stack([
-        a_real.reshape(states), a_imag.reshape(states), jnp.repeat(log_step, entries),
-        init_state[0, 0].reshape(states), init_state[0, 1].reshape(states)])
     wrows = w_out.shape[0]
     gcols, ocols = w_glu.shape[1], w_out.shape[1] // CUTS
-    copies = 2 * (len(ORDERS) + 1) * 2 * dims["z"] * dims["y"] + n_dp
+    copies = 2 * (len(ORDERS) + 3) * 2 * dims["z"] * dims["y"] + n_dp
     vmem = pl.BlockSpec(memory_space=pltpu.VMEM)
+    smem = pl.BlockSpec(memory_space=pltpu.SMEM)
     hbm = pl.BlockSpec(memory_space=pl.ANY)
     chunk = pltpu.VMEM((n_sp, rows, LANES), BF16)
     sem = pltpu.SemaphoreType.DMA
@@ -398,10 +432,10 @@
     output = pl.pallas_call(
         functools.partial(kernel, dims, (n_sp, n_dp, tokens, wd, fold, rows, states)),
         out_shape=jax.ShapeDtypeStruct((tokens, out_width), BF16),
-        in_specs=[vmem] * 8 + [hbm] * 2,
+        in_specs=[vmem] * 6 + [smem] * 2 + [vmem] * 3 + [hbm] * 2,
         out_specs=vmem,
         scratch_shapes=[
-            pltpu.VMEM(((n_dp,) if t == 0 else ()) + (2, dims["z"], dims["y"], wrows, gcols if t == 0 else ocols), BF16)
+            pltpu.VMEM(((n_dp,) if t < spread_pieces(n_dp) else ()) + (2, dims["z"], dims["y"], wrows, gcols if t == 0 else ocols), BF16)
             for t in range(len(ORDERS))
         ] + [
             pltpu.VMEM((n_dp, tokens, width), BF16),
@@ -409,6 +443,7 @@
         ] + [chunk] * 4 + [
             pltpu.VMEM((6, n_sp, states), F32),
             pltpu.VMEM((2 * fold, LANES, states), BF16),
+            pltpu.VMEM((2, wd, states), F32),
             sem((8,)), sem((copies,)), sem((copies,)),
             sem((n_sp,)), sem((n_sp,)), sem((n_sp,)), sem((n_sp,)),
             sem((n_dp,)), sem((n_dp,)), sem((n_dp, CUTS)), sem((n_dp, CUTS)),
@@ -416,8 +451,8 @@
         compiler_params=pltpu.CompilerParams(
             collective_id=0, has_side_effects=True, vmem_limit_bytes=56 * 1024 * 1024),
     )(
-        signal[0], par, pace.reshape(n_sp, 1), inm, outm, jnp.tile(skip, fold)[None],
-        b_glu[None], g_mix[None], w_glu, w_out)
+        signal[0], a_real, a_imag, init_state, in_map.transpose(0, 1, 3, 2), out_map, log_step, pace, skip,
+        b_glu, g_mix, w_glu, w_out)
     return output[None]
 
 

time: 84.2 us -> 73.2 us (0.87)
  local copies, waits for them, and re-layouts: 10.3 us -> 2.29 us
  Pallas kernels: 72.8 us -> 69.8 us
    another operation x8 -> x0, local copies, waits for them, and re-layouts: 3.65 us -> none  [the longest x6 2.41 us: per_device(): jnp.stack([a_real.reshape(states), a_imag.reshape(states), jnp.repeat(log...]
    pallas_call x1, Pallas kernels: 72.8 us -> 69.8 us  [per_device(): pl.pallas_call(functools.partial(kernel, dims, (n_sp, n_dp, tokens, wd, f...]
    reshape x1 -> x0, local copies, waits for them, and re-layouts: 1.32 us -> none  [per_device(): pace.reshape(n_sp, 1)]
    unnamed x5 -> x1, local copies, waits for them, and re-layouts: 3.12 us -> 2.29 us
where the time goes in v3:
time: 73.2 us; the launch traced here: 72.1 us
  Pallas kernels  69.8 us (95%)
  local copies, waits for them, and re-layouts  2.29 us (3%)
    pallas_call x1, Pallas kernels, per_device(): pl.pallas_call(functools.partial(kernel, dims, (n_sp, n_dp, tokens, wd, f...  69.8 us
    unnamed x1, local copies, waits for them, and re-layouts  2.29 us

profile of v3, /device:TPU:0, one launch (start us, length us, event | category | flops | bytes accessed | tf_op | source)
XLA Modules:
  0.0 72.1 jit_solution(1731680581570871639)
XLA Ops:
  0.0 69.8 %shard_map.127 = bf16[128,4096]{1,0:T(8,128)(2,1)} custom-call(bf16[128,1024]{1,0:T(8,128)(2,1)} %bitcast.4, f32[4,64]{1,0:T(4,128)} %a_real.1, f32[4,64]{1,0:T(4,128)} %a_imag.1, f32[1,2,4,64]{3,2,1,0:T(4,128)} %init.1, f32[4,2,16,64]{3,2,1,0:T(8,128)} %bitcast.5, f32[4,2,16,64]{3,2,1,0:T(8,128)} %out_map.1, f32[4]{0:T(128)} %log_step.1, f32[1,16]{1,0:T(1,128)} %pace.1, ...), custom_call_target="tpu_custom_call" | custom-call | tf_op jit(solution)/shard_map/pallas_call | solution.py:432
  69.8 2.3 %copy.15 = bf16[1,128,4096]{2,1,0:T(8,128)(2,1)} copy(bf16[1,128,4096]{2,1,0:T(8,128)(2,1)} %bitcast.3) | data formatting | bytes 2097152
